TPU v7x, 32 devices: a whole 2x2x4 slice. The times are simulated.
32 devices in a mesh: sp: 8 (over z, core), tp: 4 (over y, x).
Axes of the slice: x: 2, y: 2, z: 4, core: 2. Of those that a mesh axis runs over, the one named last changes fastest.
Arguments:
- residual: bfloat16 [1536, 2048], P('sp'), may hold values from -6 to 6
- query_in: bfloat16 [1536, 2048], P('sp', 'tp'), may hold values from -6 to 6
- value_in: bfloat16 [1536, 2048], P('sp', 'tp'), may hold values from -6 to 6
- forget_fwd: bfloat16 [1536, 2048], P('sp', 'tp'), may hold values from -4.5 to 4.5
- forget_bwd: bfloat16 [1536, 2048], P('sp', 'tp'), may hold values from -4.5 to 4.5
- jumps: float32 [16, 1536], P('tp', 'sp'), may hold values from -2.8 to 0
- gate_gap: float32 [2, 2048], P(None, 'tp'), may hold values from 0 to 0.1
- out_gate: bfloat16 [1536, 2048], P('sp', 'tp'), may hold values from -6 to 6
- head_gain: float32 [2048], P('tp'), may hold values from 0.1 to 1.9
- out_weight: bfloat16 [2048, 2048], P('tp'), may hold values from -0.25 to 0.25
- norm_gain: float32 [2048], replicated, may hold values from 0.1 to 1.9
- route_ids: int32 [1536, 4], P('sp'), may hold values from 0 to 31, all different within a row; in each aligned block of 192 rows (0 to 191, 192 to 383, ...) at most 36 rows name the same one
- route_weights: float32 [1536, 4], P('sp'), may hold values from 0.05 to 0.5
- w_gate: bfloat16 [32, 2048, 4096], P('sp', None, 'tp'), may hold values from -0.375 to 0.375
- w_up: bfloat16 [32, 2048, 4096], P('sp', None, 'tp'), may hold values from -0.375 to 0.375
- w_down: bfloat16 [32, 4096, 2048], P('sp', None, 'tp'), may hold values from -0.09375 to 0.09375
Outputs:
- mixed: bfloat16 [1536, 2048], P('sp', 'tp')
Inputs may be any that keep to these rules, and one draw needn't show every extreme that they name: `route_ids`: in each aligned block of 192 rows each expert is named by at most 36 rows, and by exactly 36 in some block; each row names 4 different experts.
All inputs are finite; a program needn't handle non-finite values.
Results may differ from a plain program's by a relative error of at most 0.024.
Values may be sent and summed in bfloat16 or wider, within the bound.
A program may use at most 128 MiB of HBM per device.

v0:
```python
import math
import jax
import jax.numpy as jnp
from jax import lax
from jax.sharding import PartitionSpec as P

EXPERTS = 32
CAP = 36
highest_precision = lax.Precision.HIGHEST
eps_norm = 1e-06
limit_value = 7.0
alpha_value = 1.702


def entering(x, axis, join, neutral, backward):
    count = lax.axis_size(axis)
    place = lax.axis_index(axis)
    ahead = count - 1 - place if backward else place
    gathered = jax.tree.map(
        lambda a, kind: lax.all_gather(a.astype(kind), axis),
        x,
        jax.tree.map(lambda a: jnp.bfloat16 if a.dtype == jnp.float32 else a.dtype, x),
    )
    state = jax.tree.map(lambda a, e: jnp.zeros_like(a) + jnp.asarray(e, a.dtype), x, neutral)

    def one(hop, state):
        source = count - 1 - hop if backward else hop
        return join(
            state,
            jax.tree.map(
                lambda a, own: lax.dynamic_index_in_dim(a, source, 0, False).astype(own.dtype),
                gathered,
                x,
            ),
        )

    return lax.fori_loop(0, ahead, one, state)


def block_pass(queries, keys_in, values, logs):
    head_rows, head_count, head_width = queries.shape
    block_size = math.gcd(head_rows, 64)
    block_count = head_rows // block_size

    def to_blocks(array):
        return array.reshape(block_count, block_size, head_count, array.shape[-1])

    q_block, k_block, v_block, log_block = (
        to_blocks(queries),
        to_blocks(keys_in),
        to_blocks(values),
        to_blocks(logs),
    )
    decay_sums = jnp.cumsum(log_block, axis=1)
    middle = decay_sums[:, block_size // 2 - 1 : block_size // 2]
    scores = jnp.einsum(
        "nthk,nshk->nhts",
        q_block * jnp.exp(decay_sums - middle),
        k_block * jnp.exp(middle - decay_sums),
        precision=highest_precision,
    )
    lower_mask = jnp.tril(jnp.ones((block_size, block_size), bool))
    within = jnp.einsum(
        "nhts,nshv->nthv", jnp.where(lower_mask, scores, 0.0), v_block, precision=highest_precision
    )
    block_end = decay_sums[:, -1]
    q_start = q_block * jnp.exp(decay_sums)
    k_end = k_block * jnp.exp(block_end[:, None] - decay_sums)

    def advance(current_state, block_items):
        query_segment, key_segment, value_segment, decay_part = block_items
        state_readout = jnp.einsum(
            "qwe,wei->qwi", query_segment, current_state, precision=highest_precision
        )
        current_state = current_state * jnp.exp(decay_part)[:, :, None] + jnp.einsum(
            "foj,fox->ojx", key_segment, value_segment, precision=highest_precision
        )
        return (current_state, state_readout)

    zero_state = jnp.zeros((head_count, head_width, values.shape[-1]), jnp.float32)
    final_state, across = lax.scan(advance, zero_state, (q_start, k_end, v_block, block_end))
    return ((within + across).reshape(head_rows, head_count, -1), final_state)


def combine_states(first_part, second_part):
    return (
        first_part[0] * second_part[0],
        second_part[0][:, :, None] * first_part[1] + second_part[1],
    )


def carried(queries, logs, running_state):
    decayed_state = queries * jnp.exp(jnp.cumsum(logs, axis=0))
    return jnp.einsum("una,nae->une", decayed_state, running_state, precision=highest_precision)


def shards(
    residual,
    query_in,
    value_in,
    forget_fwd,
    forget_bwd,
    jumps,
    gate_gap,
    out_gate,
    head_gain,
    out_weight,
    norm_gain,
    route_ids,
    route_weights,
    w_gate,
    w_up,
    w_down,
):
    head_rows, local_width = query_in.shape
    head_count = jumps.shape[0]
    head_width = local_width // head_count

    def by_head(array):
        return array.astype(jnp.float32).reshape(head_rows, head_count, head_width)

    queries = jax.nn.silu(by_head(query_in))
    values = by_head(value_in)
    jump_rows = jnp.transpose(jumps)[:, :, None]

    def gate_terms(forget_in, gap):
        key_share = gap.reshape(head_count, head_width) * jax.nn.sigmoid(-by_head(forget_in))
        return (key_share, jnp.log1p(-key_share) + jump_rows)

    keys_fwd, logs_fwd = gate_terms(forget_fwd, gate_gap[0])
    keys_bwd, logs_bwd = gate_terms(forget_bwd, gate_gap[1])
    ones_part = jnp.ones((head_count, head_width), jnp.float32)
    zero_part = jnp.zeros((head_count, head_width, head_width), jnp.float32)
    local_fwd, final_fwd = block_pass(queries, keys_fwd, values, logs_fwd)
    summary_fwd = (jnp.exp(jnp.sum(logs_fwd, axis=0)), final_fwd)
    carry_fwd = entering(summary_fwd, "sp", combine_states, (ones_part, zero_part), False)[1]
    flip_queries = jnp.flip(queries, 0)
    flip_logs = jnp.flip(logs_bwd, 0)
    local_bwd, final_bwd = block_pass(
        flip_queries, jnp.flip(keys_bwd, 0), jnp.flip(values, 0), flip_logs
    )
    summary_bwd = (jnp.exp(jnp.sum(logs_bwd, axis=0)), final_bwd)
    carry_bwd = entering(summary_bwd, "sp", combine_states, (ones_part, zero_part), True)[1]
    forward_out = local_fwd + carried(queries, logs_fwd, carry_fwd)
    backward_out = jnp.flip(local_bwd + carried(flip_queries, flip_logs, carry_bwd), 0)
    mixed_heads = forward_out + backward_out
    mean_square = jnp.mean(mixed_heads * mixed_heads, axis=-1, keepdims=True)
    normed = (mixed_heads * lax.rsqrt(mean_square + eps_norm)).reshape(head_rows, local_width)
    gated = (normed * head_gain * jax.nn.silu(out_gate.astype(jnp.float32))).astype(jnp.bfloat16)
    head_terms = jnp.dot(gated, out_weight, preferred_element_type=jnp.float32)
    summed = lax.psum(head_terms.astype(jnp.bfloat16), "tp").astype(jnp.float32)
    stream = (residual.astype(jnp.float32) + summed).astype(jnp.bfloat16)
    stream_f = stream.astype(jnp.float32)
    row_scale = lax.rsqrt(jnp.mean(stream_f * stream_f, axis=-1, keepdims=True) + eps_norm)
    normed_rows = (stream_f * row_scale * norm_gain).astype(jnp.bfloat16)
    top_count = route_ids.shape[1]
    flat_ids = route_ids.reshape(-1)
    one_hot = (flat_ids[:, None] == jnp.arange(EXPERTS, dtype=jnp.int32)[None, :]).astype(jnp.int32)
    slot_rank = jnp.sum((jnp.cumsum(one_hot, axis=0) - 1) * one_hot, axis=1)
    slot_index = flat_ids * CAP + slot_rank
    owner_rows = jnp.arange(head_rows * top_count, dtype=jnp.int32) // top_count
    slot_rows = jnp.full((EXPERTS * CAP,), head_rows, jnp.int32).at[slot_index].set(owner_rows)
    padded_rows = jnp.concatenate(
        [normed_rows, jnp.zeros((1, normed_rows.shape[1]), jnp.bfloat16)], axis=0
    )
    tp_index = lax.axis_index("tp")
    part_width = w_down.shape[2]
    column_rows = lax.dynamic_slice_in_dim(padded_rows, tp_index * part_width, part_width, 1)
    buffer = column_rows[slot_rows].reshape(EXPERTS, CAP, part_width)
    arrived = lax.all_to_all(buffer, "sp", split_axis=0, concat_axis=1, tiled=True)
    piece = lax.all_gather(arrived, "tp", axis=2, tiled=True)
    gate_sum = jnp.einsum("esd,edf->esf", piece, w_gate, preferred_element_type=jnp.float32)
    up_sum = jnp.einsum("esd,edf->esf", piece, w_up, preferred_element_type=jnp.float32)
    gate_sum = jnp.minimum(gate_sum, limit_value)
    up_sum = jnp.clip(up_sum, -limit_value, limit_value)
    active = (gate_sum * jax.nn.sigmoid(alpha_value * gate_sum) * (up_sum + 1.0)).astype(
        jnp.bfloat16
    )
    produced = jnp.einsum(
        "esf,efd->esd",
        lax.all_gather(active, "tp", axis=2, tiled=True),
        w_down,
        preferred_element_type=jnp.float32,
    ).astype(jnp.bfloat16)
    returned = lax.all_to_all(produced, "sp", split_axis=1, concat_axis=0, tiled=True)
    picked = returned.reshape(EXPERTS * CAP, part_width)[slot_index].astype(jnp.float32)
    picked = picked.reshape(head_rows, top_count, part_width)
    moe_out = jnp.sum(picked * route_weights[:, :, None], axis=1)
    own_columns = lax.dynamic_slice_in_dim(stream_f, tp_index * part_width, part_width, 1)
    return (own_columns + moe_out).astype(jnp.bfloat16)


def solution(mesh):
    return jax.shard_map(
        shards,
        mesh=mesh,
        in_specs=(
            P("sp", None),
            P("sp", "tp"),
            P("sp", "tp"),
            P("sp", "tp"),
            P("sp", "tp"),
            P("tp", "sp"),
            P(None, "tp"),
            P("sp", "tp"),
            P("tp"),
            P("tp", None),
            P(),
            P("sp", None),
            P("sp", None),
            P("sp", None, "tp"),
            P("sp", None, "tp"),
            P("sp", None, "tp"),
        ),
        out_specs=P("sp", "tp"),
        check_vma=False,
    )
```

profile of v0, /device:TPU:0, one launch (start us, length us, event | category | flops | bytes accessed | tf_op | source)
XLA Modules:
  0.0 458.2 jit_solution(397519966608035810)
XLA Ops:
  8.5 2.1 fusion.27
  12.4 2.5 log-plus-one_add_fusion
  19.5 2.2 fusion.30
  25.1 1.8 rev.18
  32.4 2.7 exponential_multiply_fusion.3
  35.9 10.8 %while.55 = (s32[]{:T(128)}, f32[4,128,128]{2,1,0:T(8,128)S(1)}, f32[3,64,4,128]{3,1,2,0:T(8,128)}, f32[3,4,128]{2,1,0:T(4,128)S(1)}, f32[3,64,4,128]{3,2,1,0:T(...) while((s32[]{:T(128)}, f32[4,128,128]{2,1,0:T(8,128)S(1)}, ...), condition=%wide.region_10.11_spmd.clone, body=%wide.region_9.10_spmd.clone.sunk | while | flops 100925440 | bytes 1842288 | solution.py:81
  54.3 10.9 %while.54 = (s32[]{:T(128)}, f32[4,128,128]{2,1,0:T(8,128)S(1)}, f32[3,64,4,128]{3,1,2,0:T(8,128)}, f32[3,4,128]{2,1,0:T(4,128)S(1)}, f32[3,64,4,128]{3,2,1,0:T(...) while((s32[]{:T(128)}, f32[4,128,128]{2,1,0:T(8,128)S(1)}, ...), condition=%wide.region_2.3_spmd.clone, body=%wide.region_1.2_spmd.clone.sunk | while | flops 100925440 | bytes 2103924 | solution.py:81
  70.0 1.9 convolution_select_fusion.1
  73.4 13.7 %all_gather.29 = bf16[8,4,128]{2,1,0:T(4,128)(2,1)S(1)} all-gather(bf16[1,4,128]{2,1,0:T(4,128)(2,1)S(1)} %fusion.59), channel_id=1, replica_groups=mesh['sp'=8,'tp'=4] {'sp'}, dimensions={0}, use_global_device_ids=true | all-gather | bytes 9216 | tf_op jit(solution)/shard_map/all_gather | solution.py:20
  87.0 1.9 convolution_select_fusion
  93.3 8.7 %all_gather.26 = bf16[8,4,128]{2,1,0:T(4,128)(2,1)S(1)} all-gather(bf16[1,4,128]{2,1,0:T(4,128)(2,1)S(1)} %fusion.58), channel_id=1, replica_groups=mesh['sp'=8,'tp'=4] {'sp'}, dimensions={0}, use_global_device_ids=true | all-gather | bytes 9216 | tf_op jit(solution)/shard_map/all_gather | solution.py:20
  102.0 3.0 reduce-window.26
  105.6 7.9 %while.53 = (s32[]{:T(128)}, f32[4,128,128]{2,1,0:T(8,128)S(1)}, s32[]{:T(128)}, bf16[8,4,128]{2,1,0:T(4,128)(2,1)S(1)}, bf16[8,4,128,128]{3,2,1,0:T(8,128)(2,1)...) while((s32[]{:T(128)}, f32[4,128,128]{2,1,0:T(8,128)S(1)}, s32[]{:T(128)}, ...), condition=%wide.region_13.14_spmd, body=%wide.region_12.13_spmd.sunk | while | flops 197126 | bytes 660627 | solution.py:37
  113.6 2.2 fusion.15
  115.8 3.6 rev.20
  120.2 2.6 convolution_convert_fusion
  123.6 3.4 scatter_custom_fusion
  127.0 43.9 %all-reduce.5.cloned.1.call-done = bf16[192,2048]{1,0:T(8,128)(2,1)} async-done(((bf16[192,2048]{1,0:T(8,128)(2,1)}), bf16[192,2048]{1,0:T(8,128)(2,1)}) %all-reduce.5.cloned.1.call-update) | async-done | bytes 786448 | tf_op jit(solution)/shard_map/psum | solution.py:151
  170.9 2.7 fusion.18
  174.0 4.2 gather_fusion
  178.5 36.6 %all_to_all.33 = bf16[32,36,512]{2,1,0:T(8,128)(2,1)S(1)} all-to-all(bf16[32,36,512]{2,1,0:T(8,128)(2,1)S(1)} %reshape.243), channel_id=1, replica_groups=mesh['sp'=8,'tp'=4] {'sp'}, dimensions={0} | all-to-all | bytes 2359296 | tf_op jit(solution)/shard_map/all_to_all | solution.py:170
  217.3 54.6 %all-gather.7.cloned.1.call-done = bf16[4,288,2048]{2,1,0:T(8,128)(2,1)} async-done(((bf16[4,288,512]{2,1,0:T(8,128)(2,1)}), bf16[4,288,2048]{2,1,0:T(8,128)(2,1)}) %all-gather.7.cloned.1.call-update) | async-done | bytes 4718608 | tf_op jit(solution)/shard_map/all_gather | solution.py:171
  272.0 10.2 %fusion.64 = f32[4,288,1024]{2,1,0:T(8,128)S(1)} fusion(bf16[4,288,2048]{2,1,0:T(8,128)(2,1)} %all-gather.7.cloned.1.call-done, bf16[4,2048,1024]{2,1,0:T(8,128)(2,1)} %param.38), kind=kOutput, calls=%fused_computation.155 | convolution fusion | flops 4831838208 | bytes 26214400 | tf_op jit(solution)/shard_map/esd,edf->esf/dot_general | solution.py:173
  282.2 14.0 %multiply_convert_fusion = bf16[4,288,1024]{2,1,0:T(8,128)(2,1)} fusion(f32[4,288,1024]{2,1,0:T(8,128)S(1)} %fusion.64, bf16[4,288,2048]{2,1,0:T(8,128)(2,1)S(1)} %copy-done.24, bf16[4,2048,1024]{2,1,0:T(8,128)(2,1)} %param.37), kind=kOutput, calls=%fused_computation.36 | convolution fusion | flops 4843634688 | bytes 28573696 | tf_op jit(solution)/shard_map/esd,edf->esf/dot_general | solution.py:172
  296.2 96.4 %all-gather.9.cloned.1.call-done = bf16[4,288,4096]{2,1,0:T(8,128)(2,1)} async-done(((bf16[4,288,1024]{2,1,0:T(8,128)(2,1)}), bf16[4,288,4096]{2,1,0:T(8,128)(2,1)}) %all-gather.9.cloned.1.call-update) | async-done | bytes 9437200 | tf_op jit(solution)/shard_map/all_gather | solution.py:181
  392.6 12.5 %convolution_convert_fusion.1 = bf16[4,288,512]{2,1,0:T(8,128)(2,1)S(1)} fusion(bf16[4,288,4096]{2,1,0:T(8,128)(2,1)} %all-gather.9.cloned.1.call-done, bf16[4,4096,512]{2,1,0:T(8,128)(2,1)} %param.39), kind=kOutput, calls=%fused_computation.42 | convolution fusion | flops 4832428032 | bytes 27394048 | tf_op jit(solution)/shard_map/esf,efd->esd/dot_general | solution.py:179
  405.0 1.9 copy.132
  407.0 4.6 %all-to-all-start.1 = ((bf16[4,288,512]{2,0,1:T(4,128)(2,1)}), bf16[4,288,512]{2,0,1:T(4,128)(2,1)S(1)}, u32[]{:S(2)}, u32[]{:S(2)}) async-start(bf16[4,288,512]{2,0,1:T(4,128)(2,1)} %copy.132), calls=%async_computation.1 | async-start | bytes 2359296 | tf_op jit(solution)/shard_map/all_to_all | solution.py:185
  411.7 29.2 %all-to-all-done.1 = bf16[4,288,512]{2,0,1:T(4,128)(2,1)S(1)} async-done(((bf16[4,288,512]{2,0,1:T(4,128)(2,1)}), bf16[4,288,512]{2,0,1:T(4,128)(2,1)S(1)}, u32[]{:S(2)}, u32[]{:S(2)}) %all-to-all-start.1) | async-done | bytes 1179680 | tf_op jit(solution)/shard_map/all_to_all | solution.py:185
  441.5 3.3 gather_fusion.1
  444.8 2.6 reshape.249
  447.4 2.5 multiply_reduce_fusion
  (187 shorter events, 72.5 us)
Async XLA Ops:
  6.5 113.6 %copy-start = (bf16[512,2048]{1,0:T(8,128)(2,1)S(1)}, bf16[512,2048]{1,0:T(8,128)(2,1)}, u32[]{:S(2)}) copy-start(bf16[512,2048]{1,0:T(8,128)(2,1)} %param.33) | copy-start | bytes 6291460
  6.5 99.1 %all-gather.13.cloned.1.call-start = ((), (), s32[]{:S(2)}) async-start(), calls=%async_computation.6 | async-start | bytes 1179648 | tf_op jit(solution)/shard_map/all_gather | solution.py:20
  7.5 7.4 %copy-start.10 = (f32[192,4]{1,0:T(8,128)}, f32[192,4]{1,0:T(8,128)S(1)}, u32[]{:S(2)}) copy-start(f32[192,4]{1,0:T(8,128)S(1)} %copy.135) | copy-start | bytes 9220
  14.9 7.6 %copy-start.4 = (f32[192,4,128]{2,1,0:T(4,128)}, f32[192,4,128]{2,1,0:T(4,128)S(1)}, u32[]{:S(2)}) copy-start(f32[192,4,128]{2,1,0:T(4,128)S(1)} %get-tuple-element.371) | copy-start | bytes 1179652
  14.9 3.7 copy-start.15
  15.4 0.8 copy-start.8
  21.6 10.0 %copy-start.2 = (f32[192,4,128]{2,1,0:T(4,128)}, f32[192,4,128]{2,1,0:T(4,128)S(1)}, u32[]{:S(2)}) copy-start(f32[192,4,128]{2,1,0:T(4,128)S(1)} %get-tuple-element.370) | copy-start | bytes 1179652
  24.5 4.3 copy-start.9
  47.4 72.0 %all-gather.11.cloned.1.call-start = ((), (), s32[]{:S(2)}) async-start(), calls=%async_computation.5 | async-start | bytes 1179648 | tf_op jit(solution)/shard_map/all_gather | solution.py:20
  54.3 13.4 %copy-start.5 = (f32[192,4,128]{2,1,0:T(4,128)S(1)}, f32[192,4,128]{2,1,0:T(4,128)}, u32[]{:S(2)}) copy-start(f32[192,4,128]{2,1,0:T(4,128)} %copy-done.4) | copy-start | bytes 1179652
  54.3 14.2 %copy-start.18 = (s32[192,4]{0,1:T(4,128)S(1)}, s32[192,4]{0,1:T(4,128)}, u32[]{:S(2)}) copy-start(s32[192,4]{0,1:T(4,128)} %param.35) | copy-start | bytes 9220
  65.9 105.0 %all-reduce.5.cloned.1.call-start = ((), (), s32[]{:S(2)}) async-start(), calls=%async_computation.2 | async-start | bytes 1572864 | tf_op jit(solution)/shard_map/psum | solution.py:151
  69.3 19.6 %copy-start.13 = (f32[3,64,4,128]{3,1,2,0:T(8,128)S(1)}, f32[3,64,4,128]{3,1,2,0:T(8,128)}, u32[]{:S(2)}) copy-start(f32[3,64,4,128]{3,1,2,0:T(8,128)} %get-tuple-element.212) | copy-start | bytes 1179652
  90.2 2.1 copy-start.3
  91.8 1.5 copy-start.22
  91.8 10.2 %copy-start.17 = (s32[6,128]{1,0:T(8,128)S(1)}, s32[6,128]{1,0:T(8,128)}, u32[]{:S(2)}) copy-start(s32[6,128]{1,0:T(8,128)} %eq.29) | copy-start | bytes 9220
  91.8 13.2 %copy-start.19 = (s32[192,4]{0,1:T(4,128)S(1)}, s32[192,4]{0,1:T(4,128)}, u32[]{:S(2)}) copy-start(s32[192,4]{0,1:T(4,128)} %param.35) | copy-start | bytes 9220
  92.4 21.2 %copy-start.12 = (f32[3,64,4,128]{3,1,0,2:T(8,128)S(1)}, f32[3,64,4,128]{3,1,0,2:T(8,128)}, u32[]{:S(2)}) copy-start(f32[3,64,4,128]{3,1,0,2:T(8,128)} %copy.118) | copy-start | bytes 1179652
  115.8 3.7 copy-start.11
  119.4 0.7 copy-start.25
  120.2 2.7 copy-start.14
  120.2 3.0 copy-start.20
  120.2 3.2 copy-start.16
  120.2 50.7 %copy-start.6 = (bf16[192,2048]{1,0:T(8,128)(2,1)S(1)}, bf16[192,2048]{1,0:T(8,128)(2,1)}, u32[]{:S(2)}) copy-start(bf16[192,2048]{1,0:T(8,128)(2,1)} %param.24) | copy-start | bytes 2359300
  122.8 50.9 %copy-start.21 = (f32[2048]{0:T(1024)S(1)}, f32[2048]{0:T(1024)}, u32[]{:S(2)}) copy-start(f32[2048]{0:T(1024)} %param.34) | copy-start | bytes 24580
  122.8 149.2 %all-gather.7.cloned.1.call-start = ((), (), s32[]{:S(2)}) async-start(), calls=%async_computation.3 | async-start | bytes 5898240 | tf_op jit(solution)/shard_map/all_gather | solution.py:171
  170.9 2.7 copy-start.7
  217.1 175.5 %all-gather.9.cloned.1.call-start = ((), (), s32[]{:S(2)}) async-start(), calls=%async_computation.4 | async-start | bytes 11796480 | tf_op jit(solution)/shard_map/all_gather | solution.py:181
  272.0 10.2 %copy-start.24 = (bf16[4,288,2048]{2,1,0:T(8,128)(2,1)S(1)}, bf16[4,288,2048]{2,1,0:T(8,128)(2,1)}, u32[]{:S(2)}) copy-start(bf16[4,288,2048]{2,1,0:T(8,128)(2,1)} %all-gather.7.cloned.1.call-done) | copy-start | bytes 14155780
  405.0 6.5 %copy-start.23 = (f32[192,4]{0,1:T(4,128)S(1)}, f32[192,4]{0,1:T(4,128)}, u32[]{:S(2)}) copy-start(f32[192,4]{0,1:T(4,128)} %param.36) | copy-start | bytes 9220
  407.0 34.0 %all-to-all-start.1 = ((bf16[4,288,512]{2,0,1:T(4,128)(2,1)}), bf16[4,288,512]{2,0,1:T(4,128)(2,1)S(1)}, u32[]{:S(2)}, u32[]{:S(2)}) async-start(bf16[4,288,512]{2,0,1:T(4,128)(2,1)} %copy.132), calls=%async_computation.1 | async-start | bytes 2359296 | tf_op jit(solution)/shard_map/all_to_all | solution.py:185
  441.5 10.1 %copy-start.1 = (bf16[512,2048]{1,0:T(8,128)(2,1)S(1)}, bf16[512,2048]{1,0:T(8,128)(2,1)}, u32[]{:S(2)}) copy-start(bf16[512,2048]{1,0:T(8,128)(2,1)} %param.33) | copy-start | bytes 6291460
Sparse Core Ops, SparseCore 0:
  47.5 24.9 all-gather.12
  74.1 21.7 all-gather.10
  122.9 47.9 all-reduce.4
  217.2 54.7 all-gather.6
  296.3 96.1 all-gather.8
where the time goes:
time: 460 us; the launch traced here: 458 us
  waiting for transfers between devices  224 us (49%)
  matrix products  60.6 us (13%)
  blocking collectives  59 us (13%)
  local copies, waits for them, and re-layouts  58.7 us (13%)
  other arithmetic  36.5 us (8%)
  between operations  13.7 us (3%)
  starting transfers between devices  4.99 us (1%)
    all_gather x1, waiting for transfers between devices, shards(): lax.all_gather(active, 'tp', axis=2, tiled=True)  96.4 us
    all_gather x1, waiting for transfers between devices, shards(): piece = lax.all_gather(arrived, 'tp', axis=2, tiled=True)  54.6 us
    psum x1, waiting for transfers between devices, shards(): summed = lax.psum(head_terms.astype(jnp.bfloat16), 'tp').astype(jnp.float32)  43.9 us
    all_to_all x1, blocking collectives, shards(): lax.all_to_all(buffer, 'sp', split_axis=0, concat_axis=1, tiled=True)  36.6 us
    all_to_all x1, waiting for transfers between devices, shards(): lax.all_to_all(produced, 'sp', split_axis=1, concat_axis=0, tiled=True)  29.2 us
    all_gather x2, blocking collectives, entering(): lax.all_gather(a.astype(kind), axis)  22.4 us
    dot_general x1, matrix products, shards(): jnp.einsum('esd,edf->esf', piece, w_gate, preferred_element_type=jnp.floa...  14 us
    dot_general x1, matrix products, shards(): jnp.einsum('esf,efd->esd', lax.all_gather(active, 'tp', axis=2, tiled=Tru...  12.5 us
  transfers between devices with their start and end apart: 6, of which 4 were waited for; matrix products, arithmetic and copies ran while one was open for 12% of the time, Pallas kernels for 0%

commit v1 on v0

--- a/solution.py
+++ b/solution.py
@@ -10,6 +10,18 @@
 eps_norm = 1e-06
 limit_value = 7.0
 alpha_value = 1.702
+
+
+def product_in_turn(shard, axis, dim, term):
+    count, index, span = (lax.axis_size(axis), lax.axis_index(axis), shard.shape[dim])
+    upward = [(i, (i + 1) % count) for i in range(count)]
+    carried, subtotal = (shard, None)
+    for step in range(count):
+        following = lax.ppermute(carried, axis, upward) if step < count - 1 else None
+        absorb = term(carried, (index - step) % count * span)
+        subtotal = absorb if subtotal is None else subtotal + absorb
+        carried = following
+    return subtotal
 
 
 def entering(x, axis, join, neutral, backward):
@@ -176,11 +188,16 @@
     active = (gate_sum * jax.nn.sigmoid(alpha_value * gate_sum) * (up_sum + 1.0)).astype(
         jnp.bfloat16
     )
-    produced = jnp.einsum(
-        "esf,efd->esd",
-        lax.all_gather(active, "tp", axis=2, tiled=True),
-        w_down,
-        preferred_element_type=jnp.float32,
+    produced = product_in_turn(
+        active,
+        "tp",
+        2,
+        lambda own_block, offset: jnp.einsum(
+            "esf,efd->esd",
+            own_block,
+            lax.dynamic_slice_in_dim(w_down, offset, own_block.shape[2], axis=1),
+            preferred_element_type=jnp.float32,
+        ),
     ).astype(jnp.bfloat16)
     returned = lax.all_to_all(produced, "sp", split_axis=1, concat_axis=0, tiled=True)
     picked = returned.reshape(EXPERTS * CAP, part_width)[slot_index].astype(jnp.float32)

time: 460 us -> 516 us (1.12)
  waiting for transfers between devices: 224 us -> 273 us
    ppermute x0 -> x3, waiting for transfers between devices: none -> 145 us  [product_in_turn(): lax.ppermute(carried, axis, upward)]
    all_gather x1 -> x0, waiting for transfers between devices: 96.4 us -> none  [shards(): lax.all_gather(active, 'tp', axis=2, tiled=True)]
    dot_general x1 -> x4, matrix products: 12.5 us -> 16.7 us  [shards(): jnp.einsum('esf,efd->esd', own_block, lax.dynamic_slice_in_dim(w_down, of...]
  transfers between devices with their start and end apart: 6 -> 8, of which waited for: 4 -> 6; matrix products, arithmetic and copies ran while one was open for 12% -> 13% of each run, Pallas kernels for 0% -> 0%
where the time goes in v1:
time: 516 us; the launch traced here: 514 us
  waiting for transfers between devices  273 us (53%)
  matrix products  63.7 us (12%)
  local copies, waits for them, and re-layouts  61.4 us (12%)
  blocking collectives  59 us (11%)
  other arithmetic  36.3 us (7%)
  between operations  13.8 us (3%)
  starting transfers between devices  6.8 us (1%)
    ppermute x3, waiting for transfers between devices, product_in_turn(): lax.ppermute(carried, axis, upward)  145 us
    all_gather x1, waiting for transfers between devices, shards(): piece = lax.all_gather(arrived, 'tp', axis=2, tiled=True)  54.9 us
    psum x1, waiting for transfers between devices, shards(): summed = lax.psum(head_terms.astype(jnp.bfloat16), 'tp').astype(jnp.float32)  44 us
    all_to_all x1, blocking collectives, shards(): lax.all_to_all(buffer, 'sp', split_axis=0, concat_axis=1, tiled=True)  36.6 us
    all_to_all x1, waiting for transfers between devices, shards(): lax.all_to_all(produced, 'sp', split_axis=1, concat_axis=0, tiled=True)  29.2 us
    all_gather x2, blocking collectives, entering(): lax.all_gather(a.astype(kind), axis)  22.4 us
    dot_general x4, matrix products, shards(): jnp.einsum('esf,efd->esd', own_block, lax.dynamic_slice_in_dim(w_down, of...  16.7 us
    dot_general x1, matrix products, shards(): jnp.einsum('esd,edf->esf', piece, w_gate, preferred_element_type=jnp.floa...  13 us
  transfers between devices with their start and end apart: 8, of which 6 were waited for; matrix products, arithmetic and copies ran while one was open for 13% of the time, Pallas kernels for 0%

profile of v1, /device:TPU:0, one launch (start us, length us, event | category | flops | bytes accessed | tf_op | source)
XLA Modules:
  0.0 514.3 jit_solution(364080091677621628)
XLA Ops:
  12.4 2.5 log-plus-one_add_fusion
  19.4 2.2 fusion.40
  32.3 2.7 exponential_multiply_fusion.3
  35.8 10.7 %while.55 = (s32[]{:T(128)}, f32[4,128,128]{2,1,0:T(8,128)S(1)}, f32[3,64,4,128]{3,1,2,0:T(8,128)}, f32[3,4,128]{2,1,0:T(4,128)S(1)}, f32[3,64,4,128]{3,2,1,0:T(...) while((s32[]{:T(128)}, f32[4,128,128]{2,1,0:T(8,128)S(1)}, ...), condition=%wide.region_10.11_spmd.clone, body=%wide.region_9.10_spmd.clone.sunk | while | flops 100925440 | bytes 1842288 | solution.py:93
  54.1 10.9 %while.54 = (s32[]{:T(128)}, f32[4,128,128]{2,1,0:T(8,128)S(1)}, f32[3,64,4,128]{3,1,2,0:T(8,128)}, f32[3,4,128]{2,1,0:T(4,128)S(1)}, f32[3,64,4,128]{3,2,1,0:T(...) while((s32[]{:T(128)}, f32[4,128,128]{2,1,0:T(8,128)S(1)}, ...), condition=%wide.region_2.3_spmd.clone, body=%wide.region_1.2_spmd.clone.sunk | while | flops 100925440 | bytes 2103924 | solution.py:93
  73.2 13.7 %all_gather.26 = bf16[8,4,128]{2,1,0:T(4,128)(2,1)S(1)} all-gather(bf16[1,4,128]{2,1,0:T(4,128)(2,1)S(1)} %fusion.73), channel_id=1, replica_groups=mesh['sp'=8,'tp'=4] {'sp'}, dimensions={0}, use_global_device_ids=true | all-gather | bytes 9216 | tf_op jit(solution)/shard_map/all_gather | solution.py:32
  93.1 8.7 %all_gather.23 = bf16[8,4,128]{2,1,0:T(4,128)(2,1)S(1)} all-gather(bf16[1,4,128]{2,1,0:T(4,128)(2,1)S(1)} %fusion.72), channel_id=1, replica_groups=mesh['sp'=8,'tp'=4] {'sp'}, dimensions={0}, use_global_device_ids=true | all-gather | bytes 9216 | tf_op jit(solution)/shard_map/all_gather | solution.py:32
  101.8 3.0 reduce-window.26
  105.4 7.9 %while.53 = (s32[]{:T(128)}, f32[4,128,128]{2,1,0:T(8,128)S(1)}, s32[]{:T(128)}, bf16[8,4,128]{2,1,0:T(4,128)(2,1)S(1)}, bf16[8,4,128,128]{3,2,1,0:T(8,128)(2,1)...) while((s32[]{:T(128)}, f32[4,128,128]{2,1,0:T(8,128)S(1)}, s32[]{:T(128)}, ...), condition=%wide.region_13.14_spmd, body=%wide.region_12.13_spmd.sunk | while | flops 197126 | bytes 660627 | solution.py:49
  113.4 2.2 fusion.25
  115.6 3.6 rev.20
  120.0 2.6 convolution_convert_fusion
  123.4 3.4 scatter_custom_fusion
  126.8 44.0 %all-reduce.5.cloned.1.call-done = bf16[192,2048]{1,0:T(8,128)(2,1)} async-done(((bf16[192,2048]{1,0:T(8,128)(2,1)}), bf16[192,2048]{1,0:T(8,128)(2,1)}) %all-reduce.5.cloned.1.call-update) | async-done | bytes 786448 | tf_op jit(solution)/shard_map/psum | solution.py:163
  170.7 2.6 fusion.28
  173.7 4.2 gather_fusion
  178.3 36.6 %all_to_all.33 = bf16[32,36,512]{2,1,0:T(8,128)(2,1)S(1)} all-to-all(bf16[32,36,512]{2,1,0:T(8,128)(2,1)S(1)} %reshape.243), channel_id=1, replica_groups=mesh['sp'=8,'tp'=4] {'sp'}, dimensions={0} | all-to-all | bytes 2359296 | tf_op jit(solution)/shard_map/all_to_all | solution.py:182
  216.8 54.9 %all-gather.6.cloned.1.call-done = bf16[4,288,2048]{2,1,0:T(8,128)(2,1)} async-done(((bf16[4,288,512]{2,1,0:T(8,128)(2,1)}), bf16[4,288,2048]{2,1,0:T(8,128)(2,1)}) %all-gather.6.cloned.1.call-update) | async-done | bytes 4718608 | tf_op jit(solution)/shard_map/all_gather | solution.py:183
  271.7 10.2 %fusion.78 = f32[4,288,1024]{2,1,0:T(8,128)S(1)} fusion(bf16[4,288,2048]{2,1,0:T(8,128)(2,1)} %all-gather.6.cloned.1.call-done, bf16[4,2048,1024]{2,1,0:T(8,128)(2,1)} %param.38), kind=kOutput, calls=%fused_computation.167 | convolution fusion | flops 4831838208 | bytes 26214400 | tf_op jit(solution)/shard_map/esd,edf->esf/dot_general | solution.py:185
  281.9 13.0 %multiply_convert_fusion = bf16[4,288,1024]{2,1,0:T(8,128)(2,1)S(1)} fusion(f32[4,288,1024]{2,1,0:T(8,128)S(1)} %fusion.78, bf16[4,288,2048]{2,1,0:T(8,128)(2,1)S(1)} %copy-done.27, bf16[4,2048,1024]{2,1,0:T(8,128)(2,1)} %param.37), kind=kOutput, calls=%fused_computation.36 | convolution fusion | flops 4843634688 | bytes 28573696 | tf_op jit(solution)/shard_map/esd,edf->esf/dot_general | solution.py:184
  297.8 52.2 %collective-permute-done = bf16[4,288,1024]{2,1,0:T(8,128)(2,1)S(1)} collective-permute-done((bf16[4,288,1024]{2,1,0:T(8,128)(2,1)S(1)}, bf16[4,288,1024]{2,1,0:T(8,128)(2,1)S(1)}, u32[]{:S(2)}, u32[]{:S(2)}) %collective-permute-start) | collective-permute-done | bytes 2359328 | tf_op jit(solution)/shard_map/ppermute | solution.py:20
  352.1 52.4 %collective-permute-done.1 = bf16[4,288,1024]{2,1,0:T(8,128)(2,1)} collective-permute-done((bf16[4,288,1024]{2,1,0:T(8,128)(2,1)S(1)}, bf16[4,288,1024]{2,1,0:T(8,128)(2,1)}, u32[]{:S(2)}, u32[]{:S(2)}) %collective-permute-start.1) | collective-permute-done | bytes 2359328 | tf_op jit(solution)/shard_map/ppermute | solution.py:20
  404.5 4.4 fusion.19
  408.9 3.6 fusion.17
  412.5 4.3 fusion.15
  416.8 40.0 %collective-permute-done.2 = bf16[4,288,1024]{2,1,0:T(8,128)(2,1)} collective-permute-done((bf16[4,288,1024]{2,1,0:T(8,128)(2,1)}, bf16[4,288,1024]{2,1,0:T(8,128)(2,1)}, u32[]{:S(2)}, u32[]{:S(2)}) %collective-permute-start.2) | collective-permute-done | bytes 2359328 | tf_op jit(solution)/shard_map/ppermute | solution.py:20
  456.8 4.4 add_convert_fusion
  463.1 4.6 all-to-all-start.1
  467.9 29.2 %all-to-all-done.1 = bf16[4,288,512]{2,0,1:T(4,128)(2,1)S(1)} async-done(((bf16[4,288,512]{2,0,1:T(4,128)(2,1)}), bf16[4,288,512]{2,0,1:T(4,128)(2,1)S(1)}, u32[]{:S(2)}, u32[]{:S(2)}) %all-to-all-start.1) | async-done | bytes 1179680 | tf_op jit(solution)/shard_map/all_to_all | solution.py:202
  497.7 3.3 gather_fusion.1
  501.0 2.6 reshape.249
  503.6 2.5 multiply_reduce_fusion
  (199 shorter events, 86.5 us)
Async XLA Ops:
  6.5 113.4 %copy-start = (bf16[512,2048]{1,0:T(8,128)(2,1)S(1)}, bf16[512,2048]{1,0:T(8,128)(2,1)}, u32[]{:S(2)}) copy-start(bf16[512,2048]{1,0:T(8,128)(2,1)} %param.33) | copy-start | bytes 6291460
  6.5 98.9 %all-gather.10.cloned.1.call-start = ((), (), s32[]{:S(2)}) async-start(), calls=%async_computation.5 | async-start | bytes 1179648 | tf_op jit(solution)/shard_map/all_gather | solution.py:32
  7.5 7.4 %copy-start.13 = (f32[192,4]{1,0:T(8,128)}, f32[192,4]{1,0:T(8,128)S(1)}, u32[]{:S(2)}) copy-start(f32[192,4]{1,0:T(8,128)S(1)} %copy.135) | copy-start | bytes 9220
  14.8 7.7 %copy-start.4 = (f32[192,4,128]{2,1,0:T(4,128)}, f32[192,4,128]{2,1,0:T(4,128)S(1)}, u32[]{:S(2)}) copy-start(f32[192,4,128]{2,1,0:T(4,128)S(1)} %get-tuple-element.371) | copy-start | bytes 1179652
  14.9 3.7 copy-start.18
  21.6 9.9 %copy-start.2 = (f32[192,4,128]{2,1,0:T(4,128)}, f32[192,4,128]{2,1,0:T(4,128)S(1)}, u32[]{:S(2)}) copy-start(f32[192,4,128]{2,1,0:T(4,128)S(1)} %get-tuple-element.370) | copy-start | bytes 1179652
  24.4 4.3 copy-start.12
  47.2 72.0 %all-gather.8.cloned.1.call-start = ((), (), s32[]{:S(2)}) async-start(), calls=%async_computation.4 | async-start | bytes 1179648 | tf_op jit(solution)/shard_map/all_gather | solution.py:32
  54.1 13.4 %copy-start.5 = (f32[192,4,128]{2,1,0:T(4,128)S(1)}, f32[192,4,128]{2,1,0:T(4,128)}, u32[]{:S(2)}) copy-start(f32[192,4,128]{2,1,0:T(4,128)} %copy-done.4) | copy-start | bytes 1179652
  54.1 14.2 %copy-start.21 = (s32[192,4]{0,1:T(4,128)S(1)}, s32[192,4]{0,1:T(4,128)}, u32[]{:S(2)}) copy-start(s32[192,4]{0,1:T(4,128)} %param.35) | copy-start | bytes 9220
  65.7 105.0 %all-reduce.5.cloned.1.call-start = ((), (), s32[]{:S(2)}) async-start(), calls=%async_computation.2 | async-start | bytes 1572864 | tf_op jit(solution)/shard_map/psum | solution.py:163
  69.1 19.6 %copy-start.16 = (f32[3,64,4,128]{3,1,2,0:T(8,128)S(1)}, f32[3,64,4,128]{3,1,2,0:T(8,128)}, u32[]{:S(2)}) copy-start(f32[3,64,4,128]{3,1,2,0:T(8,128)} %get-tuple-element.212) | copy-start | bytes 1179652
  90.0 2.1 copy-start.3
  91.6 10.2 %copy-start.20 = (s32[6,128]{1,0:T(8,128)S(1)}, s32[6,128]{1,0:T(8,128)}, u32[]{:S(2)}) copy-start(s32[6,128]{1,0:T(8,128)} %eq.34) | copy-start | bytes 9220
  91.6 13.2 %copy-start.22 = (s32[192,4]{0,1:T(4,128)S(1)}, s32[192,4]{0,1:T(4,128)}, u32[]{:S(2)}) copy-start(s32[192,4]{0,1:T(4,128)} %param.35) | copy-start | bytes 9220
  92.2 21.2 %copy-start.15 = (f32[3,64,4,128]{3,1,0,2:T(8,128)S(1)}, f32[3,64,4,128]{3,1,0,2:T(8,128)}, u32[]{:S(2)}) copy-start(f32[3,64,4,128]{3,1,0,2:T(8,128)} %copy.118) | copy-start | bytes 1179652
  115.6 3.7 copy-start.14
  120.0 2.7 copy-start.17
  120.0 3.0 copy-start.23
  120.0 3.2 copy-start.19
  120.0 50.7 %copy-start.6 = (bf16[192,2048]{1,0:T(8,128)(2,1)S(1)}, bf16[192,2048]{1,0:T(8,128)(2,1)}, u32[]{:S(2)}) copy-start(bf16[192,2048]{1,0:T(8,128)(2,1)} %param.24) | copy-start | bytes 2359300
  122.6 50.8 %copy-start.24 = (f32[2048]{0:T(1024)S(1)}, f32[2048]{0:T(1024)}, u32[]{:S(2)}) copy-start(f32[2048]{0:T(1024)} %param.34) | copy-start | bytes 24580
  122.6 149.1 %all-gather.6.cloned.1.call-start = ((), (), s32[]{:S(2)}) async-start(), calls=%async_computation.3 | async-start | bytes 5898240 | tf_op jit(solution)/shard_map/all_gather | solution.py:183
  170.7 2.6 copy-start.7
  271.7 10.2 %copy-start.27 = (bf16[4,288,2048]{2,1,0:T(8,128)(2,1)S(1)}, bf16[4,288,2048]{2,1,0:T(8,128)(2,1)}, u32[]{:S(2)}) copy-start(bf16[4,288,2048]{2,1,0:T(8,128)(2,1)} %all-gather.6.cloned.1.call-done) | copy-start | bytes 14155780
  296.3 53.7 %collective-permute-start = (bf16[4,288,1024]{2,1,0:T(8,128)(2,1)S(1)}, bf16[4,288,1024]{2,1,0:T(8,128)(2,1)S(1)}, u32[]{:S(2)}, u32[]{:S(2)}) collective-permute-start(bf16[4,288,1024]{2,1,0:T(8,128)(2,1)S(1)} %multiply_convert_fusion), channel_id=1, source_target_pairs={{0,1},{1,2},{2,3},{3,0},{4,5},{5,6},{6,7},{7,4},{8,9},{9,10},{10,1... | collective-permute-start | bytes 7077896 | tf_op jit(solution)/shard_map/ppermute | solution.py:20
  351.5 53.0 %collective-permute-start.1 = (bf16[4,288,1024]{2,1,0:T(8,128)(2,1)S(1)}, bf16[4,288,1024]{2,1,0:T(8,128)(2,1)}, u32[]{:S(2)}, u32[]{:S(2)}) collective-permute-start(bf16[4,288,1024]{2,1,0:T(8,128)(2,1)S(1)} %collective-permute-done), channel_id=1, source_target_pairs={{0,1},{1,2},{2,3},{3,0},{4,5},{5,6},{6,7},{7,4},{8,9},{9,10},{10,1... | collective-permute-start | bytes 7077896 | tf_op jit(solution)/shard_map/ppermute | solution.py:20
  404.5 52.3 %collective-permute-start.2 = (bf16[4,288,1024]{2,1,0:T(8,128)(2,1)}, bf16[4,288,1024]{2,1,0:T(8,128)(2,1)}, u32[]{:S(2)}, u32[]{:S(2)}) collective-permute-start(bf16[4,288,1024]{2,1,0:T(8,128)(2,1)} %collective-permute-done.1), channel_id=1, source_target_pairs={{0,1},{1,2},{2,3},{3,0},{4,5},{5,6},{6,7},{7,4},{8,9},{9,10},{10,1... | collective-permute-start | bytes 7077896 | tf_op jit(solution)/shard_map/ppermute | solution.py:20
  404.5 4.4 copy-start.10
  461.2 6.6 %copy-start.26 = (f32[192,4]{0,1:T(4,128)S(1)}, f32[192,4]{0,1:T(4,128)}, u32[]{:S(2)}) copy-start(f32[192,4]{0,1:T(4,128)} %param.36) | copy-start | bytes 9220
  463.1 34.0 %all-to-all-start.1 = ((bf16[4,288,512]{2,0,1:T(4,128)(2,1)}), bf16[4,288,512]{2,0,1:T(4,128)(2,1)S(1)}, u32[]{:S(2)}, u32[]{:S(2)}) async-start(bf16[4,288,512]{2,0,1:T(4,128)(2,1)} %copy.132), calls=%async_computation.1 | async-start | bytes 2359296 | tf_op jit(solution)/shard_map/all_to_all | solution.py:202
  497.7 10.1 %copy-start.1 = (bf16[512,2048]{1,0:T(8,128)(2,1)S(1)}, bf16[512,2048]{1,0:T(8,128)(2,1)}, u32[]{:S(2)}) copy-start(bf16[512,2048]{1,0:T(8,128)(2,1)} %param.33) | copy-start | bytes 6291460
  (5 other events, 5.9 us)
Sparse Core Ops, SparseCore 0:
  47.3 24.9 all-gather.9
  73.9 21.8 all-gather.7
  122.7 47.9 all-reduce.4
  216.9 54.7 all-gather.5
